TPU v7x, 768 devices: a whole 4x8x12 slice. The times are simulated.
768 devices in a mesh: sp: 16 (over y, core), dp: 48 (over z, x).
Axes of the slice: x: 4, y: 8, z: 12, core: 2. Of those that a mesh axis runs over, the one named last changes fastest.
Arguments:
- queries: bfloat16 [48, 2048, 2048], P('dp', 'sp'), may hold values from -6 to 6
- incoming_lookup_vectors: bfloat16 [48, 2048, 2048], P('dp', 'sp'), may hold values from -6 to 6
- values_in: bfloat16 [48, 2048, 2048], P('dp', 'sp'), may hold values from -6 to 6
- gates: bfloat16 [48, 2048, 2048], P('dp', 'sp'), may hold values from -6 to 6
- log_decay: float32 [48, 16, 2048], P('dp', 'sp'), may hold values from -1 to 0
- out_weight: bfloat16 [2048, 2048], P(None, 'sp'), may hold values from -0.125 to 0.125
Outputs:
- mixed: bfloat16 [48, 2048, 2048], P('dp', 'sp')
All inputs are finite; a program needn't handle non-finite values.
Results may differ from a plain program's by a relative error of at most 0.0057.
Values may be sent and summed in bfloat16 or wider, within the bound.
A program may use at most 64 MiB of HBM per device.

v0:
```python
import jax
import jax.numpy as jnp
from jax import lax
from jax.sharding import Mesh
from jax.sharding import PartitionSpec as P

BLOCK = 128
SP = ("sp_0", "sp_1")


EPS = 1e-06
ROTARY_BASE = 10000.0


def in_one_piece(arrays, axis, split_dim, concat_dim, along):
    both = jnp.concatenate(arrays, axis=along)
    result, at, outs = (
        lax.all_to_all(both, axis, split_axis=split_dim, concat_axis=concat_dim, tiled=True),
        0,
        [],
    )
    for a in arrays:
        outs.append(lax.slice_in_dim(result, at, at + a.shape[along], axis=along))
        at += a.shape[along]
    return tuple(outs)


def cut_along(shard, dim, length):
    before, after = (shard.shape[:dim], shard.shape[dim + 1 :])
    return jnp.moveaxis(shard.reshape(*before, length, -1, *after), dim, 0)


def in_order(blocks, dim):
    blocks = jnp.moveaxis(blocks, 0, dim)
    shape = blocks.shape
    return blocks.reshape(*shape[:dim], shape[dim] * shape[dim + 1], *shape[dim + 2 :])


def turned_blocks(blocks, axes, order):
    shape = [lax.axis_size(a) for a in axes]
    blocks = blocks.reshape(*shape, *blocks.shape[1:])
    for k in order:
        blocks = lax.all_to_all(blocks, axes[k], split_axis=k, concat_axis=k, tiled=True)
    return blocks.reshape(-1, *blocks.shape[len(axes) :])


def stepwise_exchange(shard, axes, order, split_dim, concat_dim):
    blocks = cut_along(shard, split_dim, lax.axis_size(axes))
    return in_order(turned_blocks(blocks, axes, order), concat_dim)


def rotary(field, head_size):
    half = head_size // 2
    inverse = ROTARY_BASE ** (-jnp.arange(half, dtype=jnp.float32) / half)
    angle = jnp.arange(field.shape[0], dtype=jnp.float32)[:, None] * inverse
    cosine = jnp.cos(angle)[:, None, :]
    sine = jnp.sin(angle)[:, None, :]
    first = field[..., :half]
    latter_operand = field[..., half:]
    return jnp.concatenate(
        [first * cosine - latter_operand * sine, first * sine + latter_operand * cosine], axis=-1
    )


def retain(query, keyed, value_rows, decay, span):
    length, heads, size = query.shape
    blocks = length // span
    high = lax.Precision.HIGHEST
    qb = query.reshape(blocks, span, heads, size).transpose(2, 0, 1, 3)
    kb = keyed.reshape(blocks, span, heads, size).transpose(2, 0, 1, 3)
    vb = value_rows.reshape(blocks, span, heads, size).transpose(2, 0, 1, 3)
    summed = jnp.cumsum(decay.reshape(heads, blocks, span), axis=-1)
    spread = summed[..., :, None] - summed[..., None, :]
    place = jnp.arange(span)
    causal = place[:, None] >= place[None, :]
    weight = jnp.exp(jnp.where(causal, spread, -jnp.inf))
    scores = jnp.einsum("hnid,hnjd->hnij", qb, kb, precision=high) * weight
    inner = jnp.einsum("hnij,hnje->hnie", scores, vb, precision=high)
    final = summed[..., -1:]
    faded = kb * jnp.exp(final - summed)[..., None]
    growth = jnp.einsum("hnjd,hnje->nhde", faded, vb, precision=high)
    carried = jnp.exp(final[..., 0]).T

    def advance(state, item):
        piece, fade = item
        return (state * fade[:, None, None] + piece, state)

    start = jnp.zeros((heads, size, size), jnp.float32)
    _, earlier_positions = lax.scan(advance, start, (growth, carried))
    lifted = qb * jnp.exp(summed)[..., None]
    cross = jnp.einsum("hnid,nhde->hnie", lifted, earlier_positions, precision=high)
    return (inner + cross).transpose(1, 2, 0, 3).reshape(length, heads, size)


def per_sequence(query, keyed, value_rows, decay):
    heads = decay.shape[0]
    length = query.shape[0]
    size = query.shape[1] // heads
    qf = rotary(query.astype(jnp.float32).reshape(length, heads, size), size)
    kf = rotary(keyed.astype(jnp.float32).reshape(length, heads, size), size)
    vf = value_rows.astype(jnp.float32).reshape(length, heads, size)
    result = retain(qf, kf, vf, decay, BLOCK)
    result = result * lax.rsqrt(jnp.mean(result * result, axis=-1, keepdims=True) + EPS)
    return result.reshape(length, heads * size).astype(jnp.bfloat16)


def on_device(queries, incoming_lookup_vectors, values_in, gates, log_decay, out_weight):
    q_heads, k_heads, content_per_attention = in_one_piece(
        (queries, incoming_lookup_vectors, values_in), SP, 2, 1, 0
    )
    normed = jax.vmap(per_sequence)(q_heads, k_heads, content_per_attention, log_decay)
    normed = stepwise_exchange(normed, SP, (1, 0), 1, 2)
    hidden = (normed.astype(jnp.float32) * jax.nn.silu(gates.astype(jnp.float32))).astype(
        jnp.bfloat16
    )
    return jnp.einsum(
        "btk,kd->btd",
        hidden,
        lax.all_gather(out_weight, SP, axis=1, tiled=True),
        preferred_element_type=jnp.float32,
    ).astype(jnp.bfloat16)


def solution(mesh):
    finer = Mesh(mesh.devices.reshape(8, 2, mesh.shape["dp"]), ("sp_0", "sp_1", "dp"))
    placed = (
        P("dp", SP, None),
        P("dp", SP, None),
        P("dp", SP, None),
        P("dp", SP, None),
        P("dp", SP, None),
        P(None, SP),
    )
    return jax.shard_map(
        on_device, mesh=finer, in_specs=placed, out_specs=P("dp", SP, None), check_vma=False
    )
```

profile of v0, /device:TPU:1, one launch (start us, length us, event | category | flops | bytes accessed | tf_op | source)
XLA Modules:
  0.0 173.4 jit_solution(868419297721917031)
XLA Ops:
  6.5 0.7 all-gather.2.cloned.1.call-update
  7.3 1.5 pad_maximum_fusion
  8.8 2.6 %copy.47 = bf16[3,128,2048]{1,0,2:T(4,128)(2,1)} copy(bf16[3,128,2048]{2,1,0:T(8,128)(2,1)S(1)} %pad_maximum_fusion) | data formatting | bytes 3145728 | tf_op jit(solution)/shard_map/concatenate | solution.py:16
  11.3 14.1 %all-to-all-start = ((bf16[3,128,2048]{1,0,2:T(4,128)(2,1)}), bf16[3,128,2048]{1,0,2:T(4,128)(2,1)S(1)}, u32[]{:S(2)}, u32[]{:S(2)}) async-start(bf16[3,128,2048]{1,0,2:T(4,128)(2,1)} %copy.47), calls=%async_computation | async-start | bytes 4194304 | tf_op jit(solution)/shard_map/all_to_all | solution.py:18
  26.1 59.6 %all-to-all-done = bf16[3,128,2048]{1,0,2:T(4,128)(2,1)S(1)} async-done(((bf16[3,128,2048]{1,0,2:T(4,128)(2,1)}), bf16[3,128,2048]{1,0,2:T(4,128)(2,1)S(1)}, u32[]{:S(2)}, u32[]{:S(2)}) %all-to-all-start) | async-done | bytes 1572896 | tf_op jit(solution)/shard_map/all_to_all | solution.py:18
  86.2 1.0 copy-done
  87.8 4.5 %multiply_subtract_fusion = (f32[1,2048,1,64]{3,1,2,0:T(8,128)S(1)}, f32[1,2048,1,64]{3,1,2,0:T(8,128)S(1)}, f32[1,2048,1,64]{3,1,2,0:T(8,128)S(1)}, f32[1,2048,1,64]{3,1,2,0:T(8,128)S(1)}) fusion(f32[1,2048,1,128]{3,1,2,0:T(8,128)S(1)} %bitcast.57, f32[64]{0:T(128)S(1)} %multiply_power_fusion, f32[1,2048,1,128]{3,1,2,0:T(8,128)S(1)} %bitcast.56), kind=kLoop, calls=%fused_computation.24 | loop fusion | flops 1703936 | bytes 4194560 | tf_op jit(solution)/shard_map/vmap()/sub | solution.py:61
  92.9 0.8 copy-done.1
  93.7 1.3 convolution_bitcast_fusion
  95.1 2.3 %convolution_multiply_fusion = f32[16,128,128]{2,1,0:T(8,128)S(1)} fusion(f32[16,128,128]{2,1,0:T(8,128)S(1)} %bitcast.54, f32[16,128,128]{2,1,0:T(8,128)S(1)} %bitcast.53, f32[16,128]{1,0:T(8,128)S(1)} %bitcast.64, pred[128,128]{1,0:T(8,128)(4,1)S(1)} %iota_compare_fusion), kind=kOutput, calls=%fused_computation.7 | convolution fusion | flops 403439616 | bytes 3170304 | tf_op jit(solution)/shard_map/vmap(hnid,hnjd->hnij)/dot_general | solution.py:77
  97.4 1.2 fusion.16
  98.7 31.8 %while.13 = (s32[]{:T(128)}, f32[1,1,128,128]{3,2,1,0:T(8,128)S(1)}, f32[16,1,1,128,128]{4,3,2,1,0:T(8,128)}, f32[16,1,1]{0,2,1:T(1,128)S(1)}, f32[16,1,1,128,128]{4,3,2,1,0:T(8,128)S(1)}, /*index=5*/s32[]{:T(128)}, s32[]{:T(128)}) while((s32[]{:T(128)}, f32[1,1,128,128]{3,2,1,0:T(8,128)S(1)}, f32[16,1,1,128,128]{4,3,2,1,0:T(8,128)}, ...), condition=%wide.region_2.3_spmd.clone, body=%wide.region_1.2_spmd.clone.sunk | while | flops 65539 | bytes 328300 | solution.py:89
  99.3 0.6 constant_dynamic-slice_fusion.2
  100.0 0.7 bitcast_add_fusion.2
  101.3 0.6 constant_dynamic-slice_fusion.2
  101.9 0.7 bitcast_add_fusion.2
  103.3 0.6 constant_dynamic-slice_fusion.2
  103.9 0.7 bitcast_add_fusion.2
  105.3 0.6 constant_dynamic-slice_fusion.2
  105.9 0.7 bitcast_add_fusion.2
  107.3 0.6 constant_dynamic-slice_fusion.2
  107.9 0.7 bitcast_add_fusion.2
  109.3 0.6 constant_dynamic-slice_fusion.2
  109.9 0.7 bitcast_add_fusion.2
  111.3 0.6 constant_dynamic-slice_fusion.2
  111.9 0.7 bitcast_add_fusion.2
  113.2 0.6 constant_dynamic-slice_fusion.2
  113.9 0.7 bitcast_add_fusion.2
  115.2 0.6 constant_dynamic-slice_fusion.2
  115.9 0.7 bitcast_add_fusion.2
  117.2 0.6 constant_dynamic-slice_fusion.2
  117.9 0.7 bitcast_add_fusion.2
  119.2 0.6 constant_dynamic-slice_fusion.2
  119.9 0.7 bitcast_add_fusion.2
  121.2 0.6 constant_dynamic-slice_fusion.2
  121.8 0.7 bitcast_add_fusion.2
  123.2 0.6 constant_dynamic-slice_fusion.2
  123.8 0.7 bitcast_add_fusion.2
  125.2 0.6 constant_dynamic-slice_fusion.2
  125.8 0.7 bitcast_add_fusion.2
  127.2 0.6 constant_dynamic-slice_fusion.2
  127.8 0.7 bitcast_add_fusion.2
  129.2 0.6 constant_dynamic-slice_fusion.2
  129.8 0.7 bitcast_add_fusion.2
  130.5 3.4 %multiply_reduce_fusion = (f32[16,128]{1,0:T(8,128)S(1)}, f32[16,128,128]{1,2,0:T(8,128)S(1)}) fusion(f32[16,128,128]{1,2,0:T(8,128)S(1)} %fusion.16, f32[16,1,1,128,128]{4,3,2,1,0:T(8,128)} %get-tuple-element.32, f32[16,128,128]{2,1,0:T(8,128)S(1)} %bitcast.55, f32[16,128]{1,0:T(8,128)S(1)} %get-tuple-element.94), kind=kOutput, calls=%fused_computation.20 | convolution fusion | flops 403699712 | bytes 4210688 | tf_op jit(solution)/shard_map/vmap(hnid,nhde->hnie)/dot_general | solution.py:91
  134.1 5.7 %all_to_all.25 = bf16[8,2,1,128,128]{3,4,0,2,1:T(8,128)(2,1)S(1)} all-to-all(bf16[8,2,1,128,128]{3,4,0,2,1:T(8,128)(2,1)S(1)} %fusion.6), channel_id=1, replica_groups=mesh['sp_0'=8,'sp_1'=2,'dp'=48] {'sp_1'}, dimensions={1} | all-to-all | bytes 1048576 | tf_op jit(solution)/shard_map/all_to_all | solution.py:43
  139.8 20.2 %all_to_all.26 = bf16[8,2,1,128,128]{3,4,1,2,0:T(8,128)(2,1)S(1)} all-to-all(bf16[8,2,1,128,128]{3,4,1,2,0:T(8,128)(2,1)S(1)} %copy.57), channel_id=1, replica_groups=mesh['sp_0'=8,'sp_1'=2,'dp'=48] {'sp_0'}, dimensions={0} | all-to-all | bytes 1048576 | tf_op jit(solution)/shard_map/all_to_all | solution.py:43
  161.0 5.5 %fusion = bf16[1,128,2048]{2,1,0:T(8,128)(2,1)} fusion(bf16[2048,2048]{1,0:T(8,128)(2,1)} %all-gather.2.cloned.1.call-done, f32[1,128,2048]{2,1,0:T(8,128)S(1)} %copy.62, bf16[1,128,2048]{2,1,0:T(8,128)(2,1)S(1)} %copy-done.3), kind=kOutput, calls=%fused_computation.4 | convolution fusion | flops 1075838976 | bytes 10485760 | tf_op jit(solution)/shard_map/btk,kd->btd/dot_general | solution.py:116
  (42 shorter events, 13.6 us)
Async XLA Ops:
  6.5 153.9 %all-gather.2.cloned.1.call-start = ((), (), s32[]{:S(2)}) async-start(), calls=%async_computation.3 | async-start | bytes 8912896 | tf_op jit(solution)/shard_map/all_gather | solution.py:119
  11.3 14.1 %copy-start.2 = (f32[1,1,2048]{2,1,0:T(1,128)S(1)}, f32[1,1,2048]{2,1,0:T(1,128)}, u32[]{:S(2)}) copy-start(f32[1,1,2048]{2,1,0:T(1,128)} %param.12) | copy-start | bytes 24580
  11.3 74.4 %all-to-all-start = ((bf16[3,128,2048]{1,0,2:T(4,128)(2,1)}), bf16[3,128,2048]{1,0,2:T(4,128)(2,1)S(1)}, u32[]{:S(2)}, u32[]{:S(2)}) async-start(bf16[3,128,2048]{1,0,2:T(4,128)(2,1)} %copy.47), calls=%async_computation | async-start | bytes 4194304 | tf_op jit(solution)/shard_map/all_to_all | solution.py:18
  85.9 1.2 copy-start
  92.3 1.4 copy-start.1
  160.0 1.0 copy-start.3
Sparse Core Ops, SparseCore 0:
  9.7 113.2 all-gather.1
where the time goes:
time: 174 us; the launch traced here: 173 us
  waiting for transfers between devices  60.4 us (35%)
  other arithmetic  28.5 us (16%)
  blocking collectives  25.8 us (15%)
  local copies, waits for them, and re-layouts  16.7 us (10%)
  starting transfers between devices  14.1 us (8%)
  matrix products  13.9 us (8%)
  between operations  13.6 us (8%)
    all_to_all x1, waiting for transfers between devices, in_one_piece(): lax.all_to_all(both, axis, split_axis=split_dim, concat_axis=concat_dim,...  59.6 us
    all_to_all x2, blocking collectives, turned_blocks(): lax.all_to_all(blocks, axes[k], split_axis=k, concat_axis=k, tiled=True)  25.8 us
    all_to_all x1, starting transfers between devices, in_one_piece(): lax.all_to_all(both, axis, split_axis=split_dim, concat_axis=concat_dim,...  14.1 us
    add x16, other arithmetic, advance(): return (state * fade[:, None, None] + piece, state)  11 us
    dynamic_slice x16, local copies, waits for them, and re-layouts, retain(): _, earlier_positions = lax.scan(advance, start, (growth, carried))  10.3 us
    dynamic_update_slice x16, other arithmetic, retain(): _, earlier_positions = lax.scan(advance, start, (growth, carried))  10.1 us
    dot_general x1, matrix products, on_device(): jnp.einsum('btk,kd->btd', hidden, lax.all_gather(out_weight, SP, axis=1,...  5.53 us
    sub x1, other arithmetic, rotary(): first * cosine - latter_operand * sine  4.46 us
  transfers between devices with their start and end apart: 2, of which 1 were waited for; matrix products, arithmetic and copies ran while one was open for 30% of the time, Pallas kernels for 0%

commit v1 on v0

v1 whole, which is shorter than its diff:
```python
import functools
import math

import jax
import jax.numpy as jnp
from jax import lax
from jax.experimental import pallas as pl
from jax.experimental.pallas import tpu as pltpu
from jax.sharding import PartitionSpec as P

EPS = 1e-06
ROTARY_BASE = 10000.0
MESH = pl.DeviceIdType.MESH
F32, BF16 = jnp.float32, jnp.bfloat16
NX, NZ, NY = 4, 12, 8
HEADS, SIZE, TOK, HALF = 16, 128, 128, 8
SPAN = 2 * TOK
LANE = HALF * SIZE
PIECE = LANE // 4


def split(x):
    high = x.astype(BF16)
    return high, (x - high.astype(F32)).astype(BF16)


def dot(a, b, ca, cb):
    return lax.dot_general(a, b, (((ca,), (cb,)), ((), ())), preferred_element_type=F32)


def exact(a, b, ca, cb):
    return lax.dot_general(
        a,
        b,
        (((ca,), (cb,)), ((), ())),
        precision=lax.Precision.HIGHEST,
        preferred_element_type=F32,
    )


def kernel(
    q_ref, k_ref, v_ref, g_ref, ld_ref, w_ref, out_ref,
    x_buf, row_buf, dec, w_buf, cos_t, sin_t, col_buf, sum_buf, qrot, krot, inner,
    g_send, g_recv, s_send, s_recv, state, hidden, p_send, p_own, p_recv,
    load_sem, w_load_sem, row_sem, xs_sem, xr_sem, ds_sem, dr_sem, ws_sem, wr_sem,
    ys_sem, yr_sem, ns_sem, nr_sem, gs_sem, gr_sem, ss_sem, sr_sem, ps_sem, pr_sem,
):
    sp = lax.axis_index("sp")
    dp = lax.axis_index("dp")
    y, c = lax.div(sp, 2), lax.rem(sp, 2)
    z, x = lax.div(dp, NX), lax.rem(dp, NX)
    other = 1 - c
    partner = 2 * y + other
    label = lax.rem(x + 2 * z, 4)
    owner_lane, owner_slot = lax.div(sp, HALF), lax.rem(sp, HALF)
    x_up = z * NX + lax.rem(x + 1, NX)
    x_dn = z * NX + lax.rem(x + NX - 1, NX)
    z_up = lax.rem(z + 1, NZ) * NX + x
    z_dn = lax.rem(z + NZ - 1, NZ) * NX + x
    y_up = 2 * lax.rem(y + 1, NY) + c
    y_dn = 2 * lax.rem(y + NY - 1, NY) + c

    def remote(src, dst, send, recv, to_sp, to_dp):
        return pltpu.make_async_remote_copy(
            src_ref=src, dst_ref=dst, send_sem=send, recv_sem=recv,
            device_id=(to_sp, to_dp), device_id_type=MESH,
        )

    mine = pl.ds(pl.multiple_of(c * LANE, LANE), LANE)
    theirs = pl.ds(pl.multiple_of(other * LANE, LANE), LANE)
    my_rows = pl.ds(pl.multiple_of(c * TOK, TOK), TOK)
    sources = (k_ref, v_ref, q_ref, g_ref)

    row_load = pltpu.make_async_copy(ld_ref.at[0], row_buf, row_sem)
    row_load.start()
    loads = [
        pltpu.make_async_copy(ref.at[0, :, mine], x_buf.at[i, my_rows, :], load_sem.at[i])
        for i, ref in enumerate(sources)
    ]
    for copy in loads:
        copy.start()
    w_load = pltpu.make_async_copy(w_ref.at[mine, :], w_buf.at[sp], w_load_sem)
    w_load.start()

    barrier = pltpu.get_barrier_semaphore()

    def greet(step, carry):
        to = lax.rem(sp + step, 2 * NY)
        pl.semaphore_signal(barrier, inc=1, device_id=(to, dp), device_id_type=MESH)
        return carry

    lax.fori_loop(1, 2 * NY, greet, 0)
    for to in (x_up, x_dn, z_up, z_dn):
        pl.semaphore_signal(barrier, inc=1, device_id=(sp, to), device_id_type=MESH)

    lane_id = lax.broadcasted_iota(jnp.int32, (SPAN, SIZE), 1)
    place = lax.broadcasted_iota(jnp.int32, (SPAN, SIZE), 0) + y * SPAN
    freq = jnp.where(lane_id >= SIZE // 2, lane_id - SIZE // 2, lane_id).astype(F32)
    angle = place.astype(F32) * jnp.exp(freq * (-math.log(ROTARY_BASE) / (SIZE // 2)))
    cos_t[...] = jnp.cos(angle)
    sine = jnp.sin(angle)
    sin_t[...] = jnp.where(lane_id >= SIZE // 2, sine, -sine)

    pl.semaphore_wait(barrier, 2 * NY - 1 + 4)

    row_load.wait()

    def decay_copy(to_y):
        to = 2 * to_y + owner_lane
        at = pl.ds(pl.multiple_of(to_y * SPAN, SPAN), SPAN)
        return to, remote(
            row_buf.at[:, at], dec.at[owner_slot], ds_sem.at[to_y], dr_sem.at[owner_slot], to, dp
        )

    def decay_send(step, carry):
        to, copy = decay_copy(lax.rem(y + step, NY))

        @pl.when(to != sp)
        def _():
            copy.start()

        return carry

    lax.fori_loop(0, NY, decay_send, 0)

    @pl.when(owner_lane == c)
    def _():
        dec[owner_slot] = row_buf[:, pl.ds(pl.multiple_of(y * SPAN, SPAN), SPAN)]

    swaps = [
        remote(
            ref.at[0, :, theirs], x_buf.at[i, my_rows, :], xs_sem.at[i], xr_sem.at[i], partner, dp
        )
        for i, ref in enumerate(sources)
    ]
    w_swap = remote(w_ref.at[theirs, :], w_buf.at[sp], ws_sem, wr_sem, partner, dp)
    for copy in swaps[:2]:
        copy.start()
    w_swap.start()
    for copy in swaps[2:]:
        copy.start()

    def cols(j):
        return pl.ds(pl.multiple_of(j * SIZE, SIZE), SIZE)

    def turn(raw):
        return raw * cos_t[...] + pltpu.roll(raw, SIZE // 2, 1) * sin_t[...]

    def w_piece(block, start=0, size=PIECE):
        rows = pl.ds(pl.multiple_of(label * PIECE + start, 128), size)
        return w_buf.at[pl.ds(2 * block, 2), rows, :]

    def up_copy(s):
        block = lax.rem(y + NY - s, NY)
        return remote(w_piece(block), w_piece(block), ys_sem.at[s], yr_sem.at[s], y_up, dp)

    def dn_copy(s):
        block = lax.rem(y + s, NY)
        return remote(w_piece(block), w_piece(block), ys_sem.at[4 + s], yr_sem.at[4 + s], y_dn, dp)

    def spread_copies(slot, block):
        return (
            remote(w_piece(block), w_piece(block), ns_sem.at[0, slot], nr_sem.at[0, slot], sp, x_up),
            remote(w_piece(block), w_piece(block), ns_sem.at[1, slot], nr_sem.at[1, slot], sp, x_dn),
            remote(
                w_piece(block, 0, 128), w_piece(block, 0, 128),
                ns_sem.at[2, slot], nr_sem.at[2, slot], sp, z_up,
            ),
            remote(
                w_piece(block, 128, 128), w_piece(block, 128, 128),
                ns_sem.at[3, slot], nr_sem.at[3, slot], sp, z_dn,
            ),
        )

    def spread(slot, block):
        for copy in spread_copies(slot, block):
            copy.start()

    for copy in loads[:2]:
        copy.wait()
    for copy in swaps[:2]:
        copy.wait_recv()

    def turn_k(j, carry):
        krot[j] = turn(x_buf[0, :, cols(j)].astype(F32))
        return carry

    lax.fori_loop(0, HALF, turn_k, 0)

    w_load.wait()
    w_swap.wait_recv()
    up_copy(0).start()
    dn_copy(0).start()

    def decay_wait(j, carry):
        @pl.when(HALF * c + j != sp)
        def _():
            at = pl.ds(0, SPAN)
            remote(row_buf.at[:, at], dec.at[j], ds_sem.at[0], dr_sem.at[j], partner, dp).wait_recv()

        return carry

    lax.fori_loop(0, HALF, decay_wait, 0)

    up_rows = lax.broadcasted_iota(jnp.int32, (SPAN, SPAN), 0)
    up_cols = lax.broadcasted_iota(jnp.int32, (SPAN, SPAN), 1)
    causal = up_rows >= up_cols
    lower = jnp.where(causal, 1.0, 0.0).astype(F32)
    decays = jnp.concatenate([dec[j] for j in range(HALF)], axis=0)
    summed = exact(decays, lower, 1, 1)
    summed_t = exact(lower, decays, 1, 1)
    for j in range(HALF):
        sum_buf[j] = summed[j : j + 1, :]
        col_buf[j] = jnp.broadcast_to(summed_t[:, j : j + 1], (SPAN, SIZE))

    def g_copy(j):
        return remote(
            g_send.at[j], g_recv.at[y], gs_sem.at[j], gr_sem.at[y], HALF * c + j, dp
        )

    def grow(j, carry):
        col = col_buf[j]
        high, low = split(krot[j] * jnp.exp(col[SPAN - 1 :, :] - col))
        v = x_buf[1, :, cols(j)]
        piece = (dot(high, v, 0, 0) + dot(low, v, 0, 0)).astype(BF16)
        to = HALF * c + j

        @pl.when(to == sp)
        def _():
            g_recv[y] = piece

        @pl.when(jnp.logical_and(to != sp, y != NY - 1))
        def _():
            g_send[j] = piece
            g_copy(j).start()

        return carry

    lax.fori_loop(0, HALF, grow, 0)

    def ring_step(s):
        up_copy(s - 1).wait_recv()
        if s < 4:
            up_copy(s).start()
        if s < 4:
            dn_copy(s - 1).wait_recv()
            if s < 3:
                dn_copy(s).start()
        spread(s - 1, lax.rem(y + NY - s, NY))
        if s < 4:
            spread(3 + s, lax.rem(y + s, NY))

    for copy in loads[2:]:
        copy.wait()
    for copy in swaps[2:]:
        copy.wait_recv()

    def turn_q(j, carry):
        qrot[j] = turn(x_buf[2, :, cols(j)].astype(F32))
        return carry

    lax.fori_loop(0, HALF, turn_q, 0)
    ring_step(1)

    def attend(j, carry):
        qh, ql = split(qrot[j])
        kh, kl = split(krot[j])
        score = dot(qh, kh, 1, 1) + dot(qh, kl, 1, 1) + dot(ql, kh, 1, 1)
        col = col_buf[j]
        gap = jnp.concatenate([col, col], axis=1) - sum_buf[j]
        gap = jnp.where(causal, gap, -1e30)
        ph, plow = split(score * jnp.exp(gap))
        v = x_buf[1, :, cols(j)]
        inner[j] = dot(ph, v, 1, 0) + dot(plow, v, 1, 0)
        return carry

    lax.fori_loop(0, 4, attend, 0)
    ring_step(2)
    lax.fori_loop(4, HALF, attend, 0)
    ring_step(3)

    def s_copy(to_y):
        to = 2 * to_y + owner_lane
        return to, remote(
            s_send.at[to_y], s_recv.at[owner_slot], ss_sem.at[to_y], sr_sem.at[owner_slot], to, dp
        )

    state[...] = jnp.zeros_like(state)

    @pl.when(y == 0)
    def _():
        s_recv[...] = jnp.zeros_like(s_recv)

    def scan(src, carry):
        @pl.when(jnp.logical_not(jnp.logical_and(src == y, owner_lane == c)))
        def _():
            remote(
                g_send.at[0], g_recv.at[src], gs_sem.at[0], gr_sem.at[src], partner, dp
            ).wait_recv()

        at = pl.ds(pl.multiple_of(src * SPAN, SPAN), SPAN)
        fade = jnp.exp(jnp.sum(row_buf[:, at], axis=1, keepdims=True))
        new = state[...] * fade + g_recv[src].astype(F32)
        state[...] = new
        to, copy = s_copy(src + 1)

        @pl.when(to == sp)
        def _():
            s_recv[owner_slot] = new.astype(BF16)

        @pl.when(to != sp)
        def _():
            s_send[src + 1] = new.astype(BF16)
            copy.start()

        return carry

    lax.fori_loop(0, NY - 1, scan, 0)
    ring_step(4)

    def finish(j, carry):
        @pl.when(jnp.logical_and(y > 0, HALF * c + j != sp))
        def _():
            remote(
                s_send.at[0], s_recv.at[j], ss_sem.at[0], sr_sem.at[j], partner, dp
            ).wait_recv()

        qh, ql = split(qrot[j] * jnp.exp(col_buf[j]))
        entering = s_recv[j]
        result = inner[j] + dot(qh, entering, 1, 0) + dot(ql, entering, 1, 0)
        scale = lax.rsqrt(jnp.mean(result * result, axis=1, keepdims=True) + EPS)
        gate = x_buf[3, :, cols(j)].astype(F32)
        hidden[:, cols(j)] = (result * scale * (gate / (1.0 + jnp.exp(-gate)))).astype(BF16)
        return carry

    lax.fori_loop(0, HALF, finish, 0)

    def p_copy(block):
        return remote(
            p_send.at[block], p_recv.at[block], ps_sem.at[block], pr_sem.at[block], partner, dp
        )

    their_rows = pl.ds(pl.multiple_of(other * TOK, TOK), TOK)

    def project(block):
        rhs = jnp.concatenate([w_buf[2 * block], w_buf[2 * block + 1]], axis=1)
        p_send[block] = dot(hidden[their_rows, :], rhs, 1, 0)
        p_copy(block).start()
        p_own[block] = dot(hidden[my_rows, :], rhs, 1, 0)

    def project_far(slot, block):
        for copy in spread_copies(slot, block):
            copy.wait_recv()
        project(block)

    project(y)

    def project_down(s, carry):
        project_far(s - 1, lax.rem(y + NY - s, NY))
        return carry

    def project_up(s, carry):
        project_far(3 + s, lax.rem(y + s, NY))
        return carry

    lax.fori_loop(1, 5, project_down, 0)
    lax.fori_loop(1, 4, project_up, 0)

    def gather(block, carry):
        p_copy(block).wait_recv()
        at = pl.ds(pl.multiple_of(block * SPAN, SPAN), SPAN)
        out_ref[0, :, at] = (p_own[block] + p_recv[block]).astype(BF16)
        return carry

    lax.fori_loop(0, NY, gather, 0)

    for copy in swaps:
        copy.wait_send()
    w_swap.wait_send()

    def drain_decay(to_y, carry):
        to, copy = decay_copy(to_y)

        @pl.when(to != sp)
        def _():
            copy.wait_send()

        return carry

    def drain_g(j, carry):
        @pl.when(jnp.logical_and(HALF * c + j != sp, y != NY - 1))
        def _():
            g_copy(j).wait_send()

        return carry

    def drain_s(to_y, carry):
        to, copy = s_copy(to_y)

        @pl.when(to != sp)
        def _():
            copy.wait_send()

        return carry

    def drain_spread(slot, carry):
        for copy in spread_copies(slot, y):
            copy.wait_send()
        return carry

    def drain_p(block, carry):
        p_copy(block).wait_send()
        return carry

    lax.fori_loop(0, NY, drain_decay, 0)
    lax.fori_loop(0, HALF, drain_g, 0)
    lax.fori_loop(1, NY, drain_s, 0)
    for s in range(4):
        up_copy(s).wait_send()
    for s in range(3):
        dn_copy(s).wait_send()
    lax.fori_loop(0, NY - 1, drain_spread, 0)
    lax.fori_loop(0, NY, drain_p, 0)


def on_device(q, k, v, gates, log_decay, weight):
    dma = pltpu.SemaphoreType.DMA
    vmem = pltpu.VMEM
    state_shape = (NY, SIZE, SIZE)
    return pl.pallas_call(
        kernel,
        out_shape=jax.ShapeDtypeStruct(q.shape, BF16),
        in_specs=[pl.BlockSpec(memory_space=pl.ANY)] * 6,
        out_specs=pl.BlockSpec(memory_space=pltpu.VMEM),
        scratch_shapes=[
            vmem((4, SPAN, LANE), BF16),
            vmem((1, NY * SPAN), F32),
            vmem((HALF, 1, SPAN), F32),
            vmem((HEADS, LANE, SIZE), BF16),
            vmem((SPAN, SIZE), F32),
            vmem((SPAN, SIZE), F32),
            vmem((HALF, SPAN, SIZE), F32),
            vmem((HALF, 1, SPAN), F32),
            vmem((HALF, SPAN, SIZE), F32),
            vmem((HALF, SPAN, SIZE), F32),
            vmem((HALF, SPAN, SIZE), F32),
            vmem(state_shape, BF16),
            vmem(state_shape, BF16),
            vmem(state_shape, BF16),
            vmem(state_shape, BF16),
            vmem((SIZE, SIZE), F32),
            vmem((SPAN, LANE), BF16),
            vmem((NY, TOK, SPAN), F32),
            vmem((NY, TOK, SPAN), F32),
            vmem((NY, TOK, SPAN), F32),
            dma((4,)),
            dma,
            dma,
            dma((4,)),
            dma((4,)),
            dma((NY,)),
            dma((HALF,)),
            dma,
            dma,
            dma((8,)),
            dma((8,)),
            dma((4, NY - 1)),
            dma((4, NY - 1)),
            dma((HALF,)),
            dma((NY,)),
            dma((NY,)),
            dma((HALF,)),
            dma((NY,)),
            dma((NY,)),
        ],
        compiler_params=pltpu.CompilerParams(
            collective_id=0, has_side_effects=True, vmem_limit_bytes=48 * 1024 * 1024
        ),
        name="retention",
    )(q, k, v, gates, log_decay, weight)


def solution(mesh):
    placed = (P("dp", "sp", None),) * 5 + (P(None, "sp"),)
    return jax.shard_map(
        on_device, mesh=mesh, in_specs=placed, out_specs=P("dp", "sp", None), check_vma=False
    )
```

time: 174 us -> 62 us (0.36)
  waiting for transfers between devices: 60.4 us -> 0 us
  Pallas kernels: 0 us -> 54.9 us
  other arithmetic: 28.5 us -> 0 us
  blocking collectives: 25.8 us -> 0 us
  starting transfers between devices: 14.1 us -> 0 us
  matrix products: 13.9 us -> 0 us
  between operations: 13.6 us -> 0.02 us
  local copies, waits for them, and re-layouts: 16.7 us -> 6.7 us
    all_to_all x1 -> x0, waiting for transfers between devices: 59.6 us -> none  [in_one_piece(): lax.all_to_all(both, axis, split_axis=split_dim, concat_axis=concat_dim,...]
    pallas_call x0 -> x1, Pallas kernels: none -> 54.9 us  [on_device(): pl.pallas_call(kernel, out_shape=jax.ShapeDtypeStruct(q.shape, BF16), in_...]
    all_to_all x2 -> x0, blocking collectives: 25.8 us -> none  [turned_blocks(): lax.all_to_all(blocks, axes[k], split_axis=k, concat_axis=k, tiled=True)]
    all_to_all x1 -> x0, starting transfers between devices: 14.1 us -> none  [in_one_piece(): lax.all_to_all(both, axis, split_axis=split_dim, concat_axis=concat_dim,...]
    dot_general x5 -> x0, matrix products: 13.9 us -> none  [the longest x1 5.53 us: on_device(): jnp.einsum('btk,kd->btd', hidden, lax.all_gather(out_weight, SP, axis=1,...]
    add x16 -> x0, other arithmetic: 11 us -> none  [advance(): return (state * fade[:, None, None] + piece, state)]
    dynamic_slice x16 -> x0, local copies, waits for them, and re-layouts: 10.3 us -> none  [retain(): _, earlier_positions = lax.scan(advance, start, (growth, carried))]
    dynamic_update_slice x16 -> x0, other arithmetic: 10.1 us -> none  [retain(): _, earlier_positions = lax.scan(advance, start, (growth, carried))]
  transfers between devices with their start and end apart: 2 -> 0, of which waited for: 1 -> 0; matrix products, arithmetic and copies ran while one was open for 30% -> 0% of each run, Pallas kernels for 0% -> 0%
where the time goes in v1:
time: 62 us; the launch traced here: 61.6 us
  Pallas kernels  54.9 us (89%)
  local copies, waits for them, and re-layouts  6.7 us (11%)
    pallas_call x1, Pallas kernels, on_device(): pl.pallas_call(kernel, out_shape=jax.ShapeDtypeStruct(q.shape, BF16), in_...  54.9 us
    unnamed x13, local copies, waits for them, and re-layouts  6.7 us

profile of v1, /device:TPU:1, one launch (start us, length us, event | category | flops | bytes accessed | tf_op | source)
XLA Modules:
  0.0 61.6 jit_solution(17040468881013530679)
XLA Ops:
  0.0 0.0 copy-start
  0.0 1.0 %copy-done = bf16[1,128,2048]{2,1,0:T(8,128)(2,1)S(1)} copy-done((bf16[1,128,2048]{2,1,0:T(8,128)(2,1)S(1)}, bf16[1,128,2048]{2,1,0:T(8,128)(2,1)}, u32[]{:S(2)}) %copy-start) | copy-done | bytes 524312
  1.0 0.0 copy-start.1
  1.0 1.0 %copy-done.1 = bf16[1,128,2048]{2,1,0:T(8,128)(2,1)S(1)} copy-done((bf16[1,128,2048]{2,1,0:T(8,128)(2,1)S(1)}, bf16[1,128,2048]{2,1,0:T(8,128)(2,1)}, u32[]{:S(2)}) %copy-start.1) | copy-done | bytes 524312
  2.1 0.0 copy-start.2
  2.1 1.0 %copy-done.2 = bf16[1,128,2048]{2,1,0:T(8,128)(2,1)S(1)} copy-done((bf16[1,128,2048]{2,1,0:T(8,128)(2,1)S(1)}, bf16[1,128,2048]{2,1,0:T(8,128)(2,1)}, u32[]{:S(2)}) %copy-start.2) | copy-done | bytes 524312
  3.1 0.0 copy-start.3
  3.1 1.0 %copy-done.3 = bf16[1,128,2048]{2,1,0:T(8,128)(2,1)S(1)} copy-done((bf16[1,128,2048]{2,1,0:T(8,128)(2,1)S(1)}, bf16[1,128,2048]{2,1,0:T(8,128)(2,1)}, u32[]{:S(2)}) %copy-start.3) | copy-done | bytes 524312
  4.2 0.0 copy-start.4
  4.2 1.0 %copy-done.4 = bf16[2048,128]{1,0:T(8,128)(2,1)S(1)} copy-done((bf16[2048,128]{1,0:T(8,128)(2,1)S(1)}, bf16[2048,128]{1,0:T(8,128)(2,1)}, u32[]{:S(2)}) %copy-start.4) | copy-done | bytes 524312
  5.2 0.0 copy-start.5
  5.2 0.7 %copy-done.5 = f32[1,1,2048]{2,1,0:T(1,128)S(1)} copy-done((f32[1,1,2048]{2,1,0:T(1,128)S(1)}, f32[1,1,2048]{2,1,0:T(1,128)}, u32[]{:S(2)}) %copy-start.5) | copy-done | bytes 8216
  5.9 54.9 %retention.1 = bf16[1,128,2048]{2,1,0:T(8,128)(2,1)S(1)} custom-call(bf16[1,128,2048]{2,1,0:T(8,128)(2,1)S(1)} %copy-done, bf16[1,128,2048]{2,1,0:T(8,128)(2,1)S(1)} %copy-done.1, bf16[1,128,2048]{2,1,0:T(8,128)(2,1)S(1)} %copy-done.2, bf16[1,128,2048]{2,1,0:T(8,128)(2,1)S(1)} %copy-done.3, f32[1,1,2048]{2,1,0:T(1,128)S(1)} %copy-done.5, ...), custom_call_target="tpu_custom_call" | custom-call | tf_op jit(solution)/shard_map/retention/pallas_call | solution.py:430
  60.8 0.8 %copy.8 = bf16[1,128,2048]{2,1,0:T(8,128)(2,1)} copy(bf16[1,128,2048]{2,1,0:T(8,128)(2,1)S(1)} %retention.1) | data formatting | bytes 1048576
Async XLA Ops:
  0.0 1.0 %copy-start = (bf16[1,128,2048]{2,1,0:T(8,128)(2,1)S(1)}, bf16[1,128,2048]{2,1,0:T(8,128)(2,1)}, u32[]{:S(2)}) copy-start(bf16[1,128,2048]{2,1,0:T(8,128)(2,1)} %q_ref.1) | copy-start | bytes 1572868
  1.0 1.0 %copy-start.1 = (bf16[1,128,2048]{2,1,0:T(8,128)(2,1)S(1)}, bf16[1,128,2048]{2,1,0:T(8,128)(2,1)}, u32[]{:S(2)}) copy-start(bf16[1,128,2048]{2,1,0:T(8,128)(2,1)} %k_ref.1) | copy-start | bytes 1572868
  2.1 1.0 %copy-start.2 = (bf16[1,128,2048]{2,1,0:T(8,128)(2,1)S(1)}, bf16[1,128,2048]{2,1,0:T(8,128)(2,1)}, u32[]{:S(2)}) copy-start(bf16[1,128,2048]{2,1,0:T(8,128)(2,1)} %v_ref.1) | copy-start | bytes 1572868
  3.1 1.0 %copy-start.3 = (bf16[1,128,2048]{2,1,0:T(8,128)(2,1)S(1)}, bf16[1,128,2048]{2,1,0:T(8,128)(2,1)}, u32[]{:S(2)}) copy-start(bf16[1,128,2048]{2,1,0:T(8,128)(2,1)} %g_ref.1) | copy-start | bytes 1572868
  4.2 1.0 %copy-start.4 = (bf16[2048,128]{1,0:T(8,128)(2,1)S(1)}, bf16[2048,128]{1,0:T(8,128)(2,1)}, u32[]{:S(2)}) copy-start(bf16[2048,128]{1,0:T(8,128)(2,1)} %w_ref.1) | copy-start | bytes 1572868
  5.2 0.7 %copy-start.5 = (f32[1,1,2048]{2,1,0:T(1,128)S(1)}, f32[1,1,2048]{2,1,0:T(1,128)}, u32[]{:S(2)}) copy-start(f32[1,1,2048]{2,1,0:T(1,128)} %ld_ref.1) | copy-start | bytes 24580

commit v2 on v1

v2 whole, which is shorter than its diff:
```python
import math

import jax
import jax.numpy as jnp
from jax import lax
from jax.experimental import pallas as pl
from jax.experimental.pallas import tpu as pltpu
from jax.sharding import PartitionSpec as P

EPS = 1e-06
ROTARY_BASE = 10000.0
MESH = pl.DeviceIdType.MESH
F32, BF16 = jnp.float32, jnp.bfloat16
NX, NZ, NY = 4, 12, 8
HEADS, SIZE, TOK, HALF = 16, 128, 128, 8
SPAN = 2 * TOK
LANE = HALF * SIZE
PIECE = LANE // 8


def split(x):
    high = x.astype(BF16)
    return high, (x - high.astype(F32)).astype(BF16)


def dot(a, b, ca, cb):
    return lax.dot_general(a, b, (((ca,), (cb,)), ((), ())), preferred_element_type=F32)


def kernel(
    q_ref, k_ref, v_ref, g_ref, ld_ref, w_ref, out_ref,
    x_buf, row_buf, dec, w_mine, w_buf, cos_t, sin_t, tri_buf, col_buf, sum_buf, fade_row, fade_buf,
    k_turned, inner, lift, gated, g_send, g_recv, s_send, s_recv, state, hidden, p_buf, p_send, p_recv,
    load_sem, w_load_sem, row_sem, xs_sem, xr_sem, ds_sem, dr_sem, ws_sem, wr_sem,
    fs_sem, ys_sem, yr_sem, ns_sem, nr_sem, gs_sem, gr_sem, ss_sem, sr_sem,
    ps_sem, pr_sem,
):
    sp = lax.axis_index("sp")
    dp = lax.axis_index("dp")
    y, c = lax.div(sp, 2), lax.rem(sp, 2)
    z, x = lax.div(dp, NX), lax.rem(dp, NX)
    other = 1 - c
    partner = 2 * y + other
    owner_lane, owner_slot = lax.div(sp, HALF), lax.rem(sp, HALF)
    x_up = z * NX + lax.rem(x + 1, NX)
    x_dn = z * NX + lax.rem(x + NX - 1, NX)
    z_up = lax.rem(z + 1, NZ) * NX + x
    z_dn = lax.rem(z + NZ - 1, NZ) * NX + x
    y_next = (lax.rem(y + 1, NY), lax.rem(y + NY - 1, NY))
    piece_row = (
        PIECE * lax.rem(x + 2 * z, 4),
        LANE // 2 + PIECE * lax.rem(z + 2 * x, 4),
    )

    def remote(src, dst, send, recv, to_sp, to_dp):
        return pltpu.make_async_remote_copy(
            src_ref=src, dst_ref=dst, send_sem=send, recv_sem=recv,
            device_id=(to_sp, to_dp), device_id_type=MESH,
        )

    mine = pl.ds(pl.multiple_of(c * LANE, LANE), LANE)
    theirs = pl.ds(pl.multiple_of(other * LANE, LANE), LANE)
    my_rows = pl.ds(pl.multiple_of(c * TOK, TOK), TOK)
    their_rows = pl.ds(pl.multiple_of(other * TOK, TOK), TOK)
    sources = (k_ref, v_ref, q_ref, g_ref)

    row_load = pltpu.make_async_copy(ld_ref.at[0], row_buf, row_sem)
    row_load.start()
    w_load = pltpu.make_async_copy(w_ref, w_mine, w_load_sem)
    w_load.start()
    loads = [
        pltpu.make_async_copy(ref.at[0, :, mine], x_buf.at[i, my_rows, :], load_sem.at[i])
        for i, ref in enumerate(sources)
    ]
    for copy in loads:
        copy.start()
    barrier = pltpu.get_barrier_semaphore()

    def greet(step, carry):
        to = lax.rem(sp + step, 2 * NY)
        pl.semaphore_signal(barrier, inc=1, device_id=(to, dp), device_id_type=MESH)
        return carry

    lax.fori_loop(1, 2 * NY, greet, 0)
    for to in (x_up, x_dn, z_up, z_dn):
        pl.semaphore_signal(barrier, inc=1, device_id=(sp, to), device_id_type=MESH)

    lane_id = lax.broadcasted_iota(jnp.int32, (SPAN, SIZE), 1)
    place = lax.broadcasted_iota(jnp.int32, (SPAN, SIZE), 0) + y * SPAN
    freq = jnp.where(lane_id >= SIZE // 2, lane_id - SIZE // 2, lane_id).astype(F32)
    angle = place.astype(F32) * jnp.exp(freq * (-math.log(ROTARY_BASE) / (SIZE // 2)))
    cos_t[...] = jnp.cos(angle)
    sine = jnp.sin(angle)
    sin_t[...] = jnp.where(lane_id >= SIZE // 2, sine, -sine)
    tri_rows = lax.broadcasted_iota(jnp.int32, (SPAN, SPAN), 0)
    tri_cols = lax.broadcasted_iota(jnp.int32, (SPAN, SPAN), 1)
    tri_buf[...] = jnp.where(tri_rows >= tri_cols, 1.0, 0.0).astype(BF16)

    pl.semaphore_wait(barrier, 2 * NY - 1 + 4)

    row_load.wait()

    def decay_copy(to_y):
        to = 2 * to_y + owner_lane
        at = pl.ds(pl.multiple_of(to_y * SPAN, SPAN), SPAN)
        return to, remote(
            row_buf.at[:, at], dec.at[owner_slot], ds_sem.at[to_y], dr_sem.at[owner_slot], to, dp
        )

    def decay_send(step, carry):
        to, copy = decay_copy(lax.rem(y + step, NY))

        @pl.when(to != sp)
        def _():
            copy.start()

        return carry

    lax.fori_loop(0, NY, decay_send, 0)

    @pl.when(owner_lane == c)
    def _():
        dec[owner_slot] = row_buf[:, pl.ds(pl.multiple_of(y * SPAN, SPAN), SPAN)]

    swaps = [
        remote(
            ref.at[0, :, theirs], x_buf.at[i, my_rows, :], xs_sem.at[i], xr_sem.at[i], partner, dp
        )
        for i, ref in enumerate(sources)
    ]
    for copy in swaps[:2]:
        copy.start()

    def first_copy(way, piece, lane):
        src_rows = pl.ds(pl.multiple_of(lane * LANE + piece_row[piece], PIECE), PIECE)
        dst_rows = pl.ds(pl.multiple_of(piece_row[piece], PIECE), PIECE)
        return remote(
            w_mine.at[src_rows, :], w_buf.at[sp, dst_rows, :],
            fs_sem.at[way, piece, lane], yr_sem.at[way, piece, c, 1], 2 * y_next[way] + lane, dp,
        )

    w_load.wait()
    for piece in range(2):
        for lane in range(2):
            for way in range(2):
                first_copy(way, piece, lane).start()

    for copy in swaps[2:]:
        copy.start()
    w_swap = remote(w_mine.at[theirs, :], w_buf.at[sp], ws_sem, wr_sem, partner, dp)
    w_swap.start()
    w_buf[sp] = w_mine[mine, :]

    def cols(j):
        return pl.ds(pl.multiple_of(j * SIZE, SIZE), SIZE)

    def turn(raw):
        return raw * cos_t[...] + pltpu.roll(raw, SIZE // 2, 1) * sin_t[...]

    def block_at(way, s):
        return lax.rem(y + NY - s, NY) if way == 0 else lax.rem(y + s, NY)

    def w_piece(block, piece, start=0, size=PIECE):
        rows = pl.ds(pl.multiple_of(piece_row[piece] + start, 64), size)
        return w_buf.at[pl.ds(2 * block, 2), rows, :]

    def hop_copy(way, piece, shard, s):
        rows = pl.ds(pl.multiple_of(piece_row[piece], PIECE), PIECE)
        ref = w_buf.at[2 * block_at(way, s - 1) + shard, rows, :]
        return remote(
            ref, ref, ys_sem.at[way, piece, shard, s], yr_sem.at[way, piece, shard, s],
            2 * y_next[way] + c, dp,
        )

    def spread_copies(piece, slot, block):
        whole = w_piece(block, piece)
        lower, upper = w_piece(block, piece, 0, PIECE // 2), w_piece(block, piece, PIECE // 2, PIECE // 2)
        refs = (whole, whole, lower, upper) if piece == 0 else (lower, upper, whole, whole)
        return [
            remote(ref, ref, ns_sem.at[piece, k, slot], nr_sem.at[piece, k, slot], sp, to)
            for k, (ref, to) in enumerate(zip(refs, (x_up, x_dn, z_up, z_dn)))
        ]

    def slot_of(way, s):
        return 6 if s == 4 else 3 * way + s - 1

    def ring_step(s):
        kept = [(p, w) for p in range(2) for w in range(2) if s < 4 or p == w]
        for piece, way in kept:
            for shard in range(2):
                hop_copy(way, piece, shard, s).wait_recv()
                if s < 3 or (s == 3 and piece == way):
                    hop_copy(way, piece, shard, s + 1).start()
        for piece, way in kept:
            for copy in spread_copies(piece, slot_of(way, s), block_at(way, s)):
                copy.start()

    for copy in loads[:2]:
        copy.wait()
    for copy in swaps[:2]:
        copy.wait_recv()

    def turn_k(i, carry):
        for t in range(2):
            j = 2 * i + t
            k_turned[j] = turn(x_buf[0, :, cols(j)].astype(F32)).T
        return carry

    lax.fori_loop(0, HALF // 2, turn_k, 0)
    ring_step(1)

    def decay_wait(j, carry):
        @pl.when(HALF * c + j != sp)
        def _():
            at = pl.ds(0, SPAN)
            remote(row_buf.at[:, at], dec.at[j], ds_sem.at[0], dr_sem.at[j], partner, dp).wait_recv()

        return carry

    lax.fori_loop(0, HALF, decay_wait, 0)

    decays = jnp.concatenate([dec[j] for j in range(HALF)], axis=0)
    first = decays.astype(BF16).astype(F32)
    second = (decays - first).astype(BF16).astype(F32)
    third = decays - first - second
    terms = jnp.concatenate([first, second, third], axis=0).astype(BF16)
    parts = dot(terms, tri_buf[...], 1, 1)
    summed = parts[:HALF] + parts[HALF : 2 * HALF] + parts[2 * HALF :]
    fading = jnp.exp(summed[:, SPAN - 1 :] - summed)
    for j in range(HALF):
        fade_row[j] = fading[j : j + 1, :]
        sum_buf[j] = summed[j : j + 1, :]

    def g_copy(j):
        return remote(
            g_send.at[j], g_recv.at[y], gs_sem.at[j], gr_sem.at[y], HALF * c + j, dp
        )

    def grow(i, carry):
        for t in range(4):
            j = 4 * i + t
            high, low = split(k_turned[j] * fade_row[j])
            v = x_buf[1, :, cols(j)]
            g_send[j] = (dot(high, v, 1, 0) + dot(low, v, 1, 0)).astype(BF16)
        for t in range(4):
            j = 4 * i + t
            to = HALF * c + j

            @pl.when(to == sp)
            def _(j=j):
                g_recv[y] = g_send[j]

            @pl.when(jnp.logical_and(to != sp, y != NY - 1))
            def _(j=j):
                g_copy(j).start()

        return carry

    lax.fori_loop(0, HALF // 4, grow, 0)
    ring_step(2)

    parts_t = dot(tri_buf[...], terms, 1, 1)
    summed_t = parts_t[:, :HALF] + parts_t[:, HALF : 2 * HALF] + parts_t[:, 2 * HALF :]
    for j in range(HALF):
        col_buf[j] = jnp.broadcast_to(summed_t[:, j : j + 1], (SPAN, SIZE))

    def fade_of(src, carry):
        at = pl.ds(pl.multiple_of(src * SPAN, SPAN), SPAN)
        total = jnp.exp(jnp.sum(row_buf[:, at], axis=1, keepdims=True))
        fade_buf[src] = jnp.broadcast_to(total, (1, SIZE))
        return carry

    lax.fori_loop(0, NY - 1, fade_of, 0)

    for copy in loads[2:]:
        copy.wait()
    for copy in swaps[2:]:
        copy.wait_recv()

    def attend(i, carry):
        for t in range(2):
            j = 2 * i + t
            kh, kl = split(k_turned[j])
            gate = x_buf[3, :, cols(j)].astype(F32)
            gated[j] = gate / (1.0 + jnp.exp(-gate))
            for half in range(2):
                rows = slice(half * TOK, half * TOK + TOK)
                width = TOK * (half + 1)
                raw = x_buf[2, rows, cols(j)].astype(F32)
                turned = raw * cos_t[rows, :] + pltpu.roll(raw, SIZE // 2, 1) * sin_t[rows, :]
                qh, ql = split(turned)
                near = kh[:, :width]
                score = dot(qh, near, 1, 0) + dot(ql, near, 1, 0) + dot(qh, kl[:, :width], 1, 0)
                col = col_buf[j, rows, :]
                lh, ll = split(turned * jnp.exp(col))
                lift[j, rows, :SIZE] = lh
                lift[j, rows, SIZE:] = ll
                wide = jnp.concatenate([col] * (half + 1), axis=1)
                gap = wide - sum_buf[j][:, :width]
                at = lax.broadcasted_iota(jnp.int32, (TOK, width), 0) + half * TOK
                past = at >= lax.broadcasted_iota(jnp.int32, (TOK, width), 1)
                ph, plow = split(score * jnp.exp(jnp.where(past, gap, -1e30)))
                v = x_buf[1, :width, cols(j)]
                inner[j, rows, :] = dot(ph, v, 1, 0) + dot(plow, v, 1, 0)
        return carry

    ring_step(3)
    lax.fori_loop(0, 2, attend, 0)
    ring_step(4)
    lax.fori_loop(2, 4, attend, 0)

    def s_copy(to_y):
        to = 2 * to_y + owner_lane
        return to, remote(
            s_send.at[to_y], s_recv.at[owner_slot], ss_sem.at[to_y], sr_sem.at[owner_slot], to, dp
        )

    state[...] = jnp.zeros_like(state)

    @pl.when(y == 0)
    def _():
        s_recv[...] = jnp.zeros_like(s_recv)

    def scan(src, carry):
        @pl.when(jnp.logical_not(jnp.logical_and(src == y, owner_lane == c)))
        def _():
            remote(
                g_send.at[0], g_recv.at[src], gs_sem.at[0], gr_sem.at[src], partner, dp
            ).wait_recv()

        new = state[...] * fade_buf[src] + g_recv[src].astype(F32)
        state[...] = new
        to, copy = s_copy(src + 1)

        @pl.when(to == sp)
        def _():
            s_recv[owner_slot] = new.astype(BF16)

        @pl.when(to != sp)
        def _():
            s_send[src + 1] = new.astype(BF16)
            copy.start()

        return carry

    lax.fori_loop(0, NY - 1, scan, 0)

    def finish(i, carry):
        for t in range(2):
            j = 2 * i + t

            @pl.when(jnp.logical_and(y > 0, HALF * c + j != sp))
            def _(j=j):
                remote(
                    s_send.at[0], s_recv.at[j], ss_sem.at[0], sr_sem.at[j], partner, dp
                ).wait_recv()

        for t in range(2):
            j = 2 * i + t
            entering = s_recv[j]
            result = inner[j] + dot(lift[j], jnp.concatenate([entering, entering], axis=0), 1, 0)
            scale = lax.rsqrt(jnp.mean(result * result, axis=1, keepdims=True) + EPS)
            hidden[:, cols(j)] = (result * scale * gated[j]).astype(BF16)
        return carry

    lax.fori_loop(0, HALF // 2, finish, 0)

    def p_copy(block):
        return remote(
            p_send.at[block], p_recv.at[block], ps_sem.at[block], pr_sem.at[block], partner, dp
        )

    def project(block):
        rhs = jnp.concatenate([w_buf[2 * block], w_buf[2 * block + 1]], axis=1)
        p_buf[block] = dot(hidden[...], rhs, 1, 0)
        p_send[block] = p_buf[block, their_rows, :].astype(BF16)
        p_copy(block).start()

    w_swap.wait_recv()
    project(y)

    def project_far(slot, carry):
        way, s = lax.div(slot, 3), lax.rem(slot, 3) + 1
        step = jnp.where(slot == 6, 4, jnp.where(way == 0, NY - s, s))
        block = lax.rem(y + step, NY)
        for piece in range(2):
            for copy in spread_copies(piece, slot, block):
                copy.wait_recv()
        project(block)
        return carry

    lax.fori_loop(0, NY - 1, project_far, 0)

    def gather(i, carry):
        for t in range(2):
            block = 2 * i + t
            p_copy(block).wait_recv()
            at = pl.ds(pl.multiple_of(block * SPAN, SPAN), SPAN)
            total = p_buf[block, my_rows, :] + p_recv[block].astype(F32)
            out_ref[0, :, at] = total.astype(BF16)
        return carry

    lax.fori_loop(0, NY // 2, gather, 0)

    for copy in swaps:
        copy.wait_send()
    w_swap.wait_send()

    def drain_decay(to_y, carry):
        to, copy = decay_copy(to_y)

        @pl.when(to != sp)
        def _():
            copy.wait_send()

        return carry

    def drain_g(j, carry):
        @pl.when(jnp.logical_and(HALF * c + j != sp, y != NY - 1))
        def _():
            g_copy(j).wait_send()

        return carry

    def drain_s(to_y, carry):
        to, copy = s_copy(to_y)

        @pl.when(to != sp)
        def _():
            copy.wait_send()

        return carry

    def drain_spread(slot, carry):
        for piece in range(2):
            for copy in spread_copies(piece, slot, y):
                copy.wait_send()
        return carry

    def drain_p(block, carry):
        p_copy(block).wait_send()
        return carry

    lax.fori_loop(0, NY, drain_decay, 0)
    lax.fori_loop(0, HALF, drain_g, 0)
    lax.fori_loop(1, NY, drain_s, 0)
    for piece in range(2):
        for way in range(2):
            for lane in range(2):
                first_copy(way, piece, lane).wait_send()
                for s in (2, 3, 4):
                    if s < 4 or piece == way:
                        hop_copy(way, piece, lane, s).wait_send()
    lax.fori_loop(0, NY - 1, drain_spread, 0)
    lax.fori_loop(0, NY, drain_p, 0)


def on_device(q, k, v, gates, log_decay, weight):
    dma = pltpu.SemaphoreType.DMA
    vmem = pltpu.VMEM
    state_shape = (NY, SIZE, SIZE)
    return pl.pallas_call(
        kernel,
        out_shape=pltpu.VMEM(q.shape, BF16),
        in_specs=[pl.BlockSpec(memory_space=pltpu.HBM)] * 6,
        out_specs=pl.BlockSpec(memory_space=pltpu.VMEM),
        scratch_shapes=[
            vmem((4, SPAN, LANE), BF16),
            vmem((1, NY * SPAN), F32),
            vmem((HALF, 1, SPAN), F32),
            vmem((2 * LANE, SIZE), BF16),
            vmem((HEADS, LANE, SIZE), BF16),
            vmem((SPAN, SIZE), F32),
            vmem((SPAN, SIZE), F32),
            vmem((SPAN, SPAN), BF16),
            vmem((HALF, SPAN, SIZE), F32),
            vmem((HALF, 1, SPAN), F32),
            vmem((HALF, 1, SPAN), F32),
            vmem((NY, 1, SIZE), F32),
            vmem((HALF, SIZE, SPAN), F32),
            vmem((HALF, SPAN, SIZE), F32),
            vmem((HALF, SPAN, SPAN), BF16),
            vmem((HALF, SPAN, SIZE), F32),
            vmem(state_shape, BF16),
            vmem(state_shape, BF16),
            vmem(state_shape, BF16),
            vmem(state_shape, BF16),
            vmem((SIZE, SIZE), F32),
            vmem((SPAN, LANE), BF16),
            vmem((NY, SPAN, SPAN), F32),
            vmem((NY, TOK, SPAN), BF16),
            vmem((NY, TOK, SPAN), BF16),
            dma((4,)),
            dma,
            dma,
            dma((4,)),
            dma((4,)),
            dma((NY,)),
            dma((HALF,)),
            dma,
            dma,
            dma((2, 2, 2)),
            dma((2, 2, 2, 5)),
            dma((2, 2, 2, 5)),
            dma((2, 4, NY - 1)),
            dma((2, 4, NY - 1)),
            dma((HALF,)),
            dma((NY,)),
            dma((NY,)),
            dma((HALF,)),
            dma((NY,)),
            dma((NY,)),
        ],
        compiler_params=pltpu.CompilerParams(
            collective_id=0, has_side_effects=True, vmem_limit_bytes=60 * 1024 * 1024
        ),
        name="retention",
    )(q, k, v, gates, log_decay, weight)


def solution(mesh):
    placed = (P("dp", "sp", None),) * 5 + (P(None, "sp"),)
    return jax.shard_map(
        on_device, mesh=mesh, in_specs=placed, out_specs=P("dp", "sp", None), check_vma=False
    )
```

time: 62 us -> 52.9 us (0.85)
  the two profiles are of different devices: /device:TPU:1 before, /device:TPU:18 now
where the time goes in v2:
time: 52.9 us; the launch traced here: 52.8 us
  Pallas kernels  51.9 us (98%)
  local copies, waits for them, and re-layouts  0.8 us (2%)
    pallas_call x1, Pallas kernels, on_device(): pl.pallas_call(kernel, out_shape=pltpu.VMEM(q.shape, BF16), in_specs=[pl....  51.9 us

profile of v2, /device:TPU:18, one launch (start us, length us, event | category | flops | bytes accessed | tf_op | source)
XLA Modules:
  0.0 52.8 jit_solution(17713783550816648065)
XLA Ops:
  0.0 51.9 %retention.1 = bf16[1,128,2048]{2,1,0:T(8,128)(2,1)S(1)} custom-call(bf16[1,128,2048]{2,1,0:T(8,128)(2,1)} %q_ref.1, bf16[1,128,2048]{2,1,0:T(8,128)(2,1)} %k_ref.1, bf16[1,128,2048]{2,1,0:T(8,128)(2,1)} %v_ref.1, bf16[1,128,2048]{2,1,0:T(8,128)(2,1)} %g_ref.1, f32[1,1,2048]{2,1,0:T(1,128)} %ld_ref.1, bf16[2048,128]{1,0:T(8,128)(2,1)} %w_ref.1), custom_call_target="tpu_custom_call" | custom-call | tf_op jit(solution)/shard_map/retention/pallas_call | solution.py:462
  52.0 0.8 %copy.8 = bf16[1,128,2048]{2,1,0:T(8,128)(2,1)} copy(bf16[1,128,2048]{2,1,0:T(8,128)(2,1)S(1)} %retention.1) | data formatting | bytes 1048576

commit v3 on v2

--- a/solution.py
+++ b/solution.py
@@ -304,10 +304,9 @@
                 inner[j, rows, :] = dot(ph, v, 1, 0) + dot(plow, v, 1, 0)
         return carry
 
+    lax.fori_loop(0, 2, attend, 0)
+    lax.fori_loop(2, 4, attend, 0)
     ring_step(3)
-    lax.fori_loop(0, 2, attend, 0)
-    ring_step(4)
-    lax.fori_loop(2, 4, attend, 0)
 
     def s_copy(to_y):
         to = 2 * to_y + owner_lane
@@ -344,6 +343,7 @@
         return carry
 
     lax.fori_loop(0, NY - 1, scan, 0)
+    ring_step(4)
 
     def finish(i, carry):
         for t in range(2):

time: 52.9 us -> 49.6 us (0.938)
  the two profiles are of different devices: /device:TPU:18 before, /device:TPU:1 now
where the time goes in v3:
time: 49.6 us; the launch traced here: 49.3 us
  Pallas kernels  48.5 us (98%)
  local copies, waits for them, and re-layouts  0.8 us (2%)
    pallas_call x1, Pallas kernels, on_device(): pl.pallas_call(kernel, out_shape=pltpu.VMEM(q.shape, BF16), in_specs=[pl....  48.5 us

profile of v3, /device:TPU:1, one launch (start us, length us, event | category | flops | bytes accessed | tf_op | source)
XLA Modules:
  0.0 49.3 jit_solution(9827883513355541774)
XLA Ops:
  0.0 48.5 %retention.1 = bf16[1,128,2048]{2,1,0:T(8,128)(2,1)S(1)} custom-call(bf16[1,128,2048]{2,1,0:T(8,128)(2,1)} %q_ref.1, bf16[1,128,2048]{2,1,0:T(8,128)(2,1)} %k_ref.1, bf16[1,128,2048]{2,1,0:T(8,128)(2,1)} %v_ref.1, bf16[1,128,2048]{2,1,0:T(8,128)(2,1)} %g_ref.1, f32[1,1,2048]{2,1,0:T(1,128)} %ld_ref.1, bf16[2048,128]{1,0:T(8,128)(2,1)} %w_ref.1), custom_call_target="tpu_custom_call" | custom-call | tf_op jit(solution)/shard_map/retention/pallas_call | solution.py:462
  48.5 0.8 %copy.8 = bf16[1,128,2048]{2,1,0:T(8,128)(2,1)} copy(bf16[1,128,2048]{2,1,0:T(8,128)(2,1)S(1)} %retention.1) | data formatting | bytes 1048576

commit v4 on v3

--- a/solution.py
+++ b/solution.py
@@ -98,6 +98,15 @@
 
     pl.semaphore_wait(barrier, 2 * NY - 1 + 4)
 
+    swaps = [
+        remote(
+            ref.at[0, :, theirs], x_buf.at[i, my_rows, :], xs_sem.at[i], xr_sem.at[i], partner, dp
+        )
+        for i, ref in enumerate(sources)
+    ]
+    for copy in swaps[:2]:
+        copy.start()
+
     row_load.wait()
 
     def decay_copy(to_y):
@@ -121,15 +130,6 @@
     @pl.when(owner_lane == c)
     def _():
         dec[owner_slot] = row_buf[:, pl.ds(pl.multiple_of(y * SPAN, SPAN), SPAN)]
-
-    swaps = [
-        remote(
-            ref.at[0, :, theirs], x_buf.at[i, my_rows, :], xs_sem.at[i], xr_sem.at[i], partner, dp
-        )
-        for i, ref in enumerate(sources)
-    ]
-    for copy in swaps[:2]:
-        copy.start()
 
     def first_copy(way, piece, lane):
         src_rows = pl.ds(pl.multiple_of(lane * LANE + piece_row[piece], PIECE), PIECE)
@@ -257,25 +257,6 @@
         return carry
 
     lax.fori_loop(0, HALF // 4, grow, 0)
-    ring_step(2)
-
-    parts_t = dot(tri_buf[...], terms, 1, 1)
-    summed_t = parts_t[:, :HALF] + parts_t[:, HALF : 2 * HALF] + parts_t[:, 2 * HALF :]
-    for j in range(HALF):
-        col_buf[j] = jnp.broadcast_to(summed_t[:, j : j + 1], (SPAN, SIZE))
-
-    def fade_of(src, carry):
-        at = pl.ds(pl.multiple_of(src * SPAN, SPAN), SPAN)
-        total = jnp.exp(jnp.sum(row_buf[:, at], axis=1, keepdims=True))
-        fade_buf[src] = jnp.broadcast_to(total, (1, SIZE))
-        return carry
-
-    lax.fori_loop(0, NY - 1, fade_of, 0)
-
-    for copy in loads[2:]:
-        copy.wait()
-    for copy in swaps[2:]:
-        copy.wait_recv()
 
     def attend(i, carry):
         for t in range(2):
@@ -304,9 +285,6 @@
                 inner[j, rows, :] = dot(ph, v, 1, 0) + dot(plow, v, 1, 0)
         return carry
 
-    lax.fori_loop(0, 2, attend, 0)
-    lax.fori_loop(2, 4, attend, 0)
-    ring_step(3)
 
     def s_copy(to_y):
         to = 2 * to_y + owner_lane
@@ -342,12 +320,34 @@
 
         return carry
 
+    parts_t = dot(tri_buf[...], terms, 1, 1)
+    summed_t = parts_t[:, :HALF] + parts_t[:, HALF : 2 * HALF] + parts_t[:, 2 * HALF :]
+    for j in range(HALF):
+        col_buf[j] = jnp.broadcast_to(summed_t[:, j : j + 1], (SPAN, SIZE))
+
+    def fade_of(src, carry):
+        at = pl.ds(pl.multiple_of(src * SPAN, SPAN), SPAN)
+        total = jnp.exp(jnp.sum(row_buf[:, at], axis=1, keepdims=True))
+        fade_buf[src] = jnp.broadcast_to(total, (1, SIZE))
+        return carry
+
+    lax.fori_loop(0, NY - 1, fade_of, 0)
+
+    ring_step(2)
+    for copy in loads[2:]:
+        copy.wait()
+    for copy in swaps[2:]:
+        copy.wait_recv()
+
+    lax.fori_loop(0, 2, attend, 0)
+    ring_step(3)
     lax.fori_loop(0, NY - 1, scan, 0)
+    lax.fori_loop(2, 4, attend, 0)
     ring_step(4)
 
     def finish(i, carry):
-        for t in range(2):
-            j = 2 * i + t
+        for t in range(4):
+            j = 4 * i + t
 
             @pl.when(jnp.logical_and(y > 0, HALF * c + j != sp))
             def _(j=j):
@@ -355,15 +355,15 @@
                     s_send.at[0], s_recv.at[j], ss_sem.at[0], sr_sem.at[j], partner, dp
                 ).wait_recv()
 
-        for t in range(2):
-            j = 2 * i + t
+        for t in range(4):
+            j = 4 * i + t
             entering = s_recv[j]
             result = inner[j] + dot(lift[j], jnp.concatenate([entering, entering], axis=0), 1, 0)
             scale = lax.rsqrt(jnp.mean(result * result, axis=1, keepdims=True) + EPS)
             hidden[:, cols(j)] = (result * scale * gated[j]).astype(BF16)
         return carry
 
-    lax.fori_loop(0, HALF // 2, finish, 0)
+    lax.fori_loop(0, HALF // 4, finish, 0)
 
     def p_copy(block):
         return remote(

time: 49.6 us -> 49.6 us (level)
  no operation moved by 1% of the time
where the time goes in v4:
time: 49.6 us; the launch traced here: 49.5 us
  Pallas kernels  48.7 us (98%)
  local copies, waits for them, and re-layouts  0.8 us (2%)
    pallas_call x1, Pallas kernels, on_device(): pl.pallas_call(kernel, out_shape=pltpu.VMEM(q.shape, BF16), in_specs=[pl....  48.7 us

profile of v4, /device:TPU:1, one launch (start us, length us, event | category | flops | bytes accessed | tf_op | source)
XLA Modules:
  0.0 49.5 jit_solution(115728061925817580)
XLA Ops:
  0.0 48.7 %retention.1 = bf16[1,128,2048]{2,1,0:T(8,128)(2,1)S(1)} custom-call(bf16[1,128,2048]{2,1,0:T(8,128)(2,1)} %q_ref.1, bf16[1,128,2048]{2,1,0:T(8,128)(2,1)} %k_ref.1, bf16[1,128,2048]{2,1,0:T(8,128)(2,1)} %v_ref.1, bf16[1,128,2048]{2,1,0:T(8,128)(2,1)} %g_ref.1, f32[1,1,2048]{2,1,0:T(1,128)} %ld_ref.1, bf16[2048,128]{1,0:T(8,128)(2,1)} %w_ref.1), custom_call_target="tpu_custom_call" | custom-call | tf_op jit(solution)/shard_map/retention/pallas_call | solution.py:462
  48.7 0.8 %copy.8 = bf16[1,128,2048]{2,1,0:T(8,128)(2,1)} copy(bf16[1,128,2048]{2,1,0:T(8,128)(2,1)S(1)} %retention.1) | data formatting | bytes 1048576
